TPU v7x, 128 devices: a whole 4x4x4 slice. The times are simulated.
128 devices in a mesh: sp: 16 (over z, y), tp: 8 (over x, core).
Axes of the slice: x: 4, y: 4, z: 4, core: 2. Of those that a mesh axis runs over, the one named last changes fastest.
Arguments:
- query_proj: bfloat16 [16384, 2048], P('sp', 'tp'), may hold values from -6 to 6
- key_proj: bfloat16 [16384, 2048], P('sp', 'tp'), may hold values from -6 to 6
- value_proj: bfloat16 [16384, 4096], P('sp', 'tp'), may hold values from -6 to 6
- gate_proj: bfloat16 [16384, 4096], P('sp', 'tp'), may hold values from -6 to 6
- log_decay: float32 [16384, 8], P('sp', 'tp'), may hold values from -0.75 to 0, as said below
- residual: bfloat16 [16384, 2048], P('sp'), may hold values from -4 to 4
- out_weight: bfloat16 [4096, 2048], P('tp'), may hold values from -0.09375 to 0.09375
- norm_gain: float32 [2, 2048], replicated, may hold values from 0.1 to 1.9
- norm_bias: float32 [2, 2048], replicated, may hold values from -1.5 to 1.5
- up_gate: bfloat16 [2048, 5632], P('sp', 'tp'), may hold values from -0.125 to 0.125
- up_value: bfloat16 [2048, 5632], P('sp', 'tp'), may hold values from -0.125 to 0.125
- conv_weight: float32 [2, 3, 5632], P(None, None, 'tp'), may hold values from -3 to 3
- conv_bias: float32 [2, 5632], P(None, 'tp'), may hold values from -1.5 to 1.5
- down_weight: bfloat16 [5632, 2048], P('tp', 'sp'), may hold values from -0.078125 to 0.078125
Outputs:
- layer_output: bfloat16 [16384, 2048], P(('sp', 'tp'))
Inputs may be any that keep to these rules, and one draw needn't show every extreme that they name: `log_decay`: all entries are negative.
All inputs are finite; a program needn't handle non-finite values.
Results may differ from a plain program's by a relative error of at most 0.023.
Values may be sent and summed in bfloat16 or wider, within the bound.
No kernel may reach another device: no remote copies, remote signals or barrier semaphores. Data moves between devices by JAX's collectives and lax.ppermute only.
A program may use at most 128 MiB of HBM per device.

v0:
```python
import jax
import jax.numpy as jnp
from jax import lax
from jax.sharding import Mesh
from jax.sharding import PartitionSpec as P

BLOCK = 256
SP = ("sp_0", "sp_1")
SP_TP = ("sp_0", "sp_1", "tp")


alpha_scale = 8.0**0.25
rope_base = 10000.0
tiny_stabilizer = 1e-05


def turned_gather(arrays, axis, dims):
    turned = [jnp.moveaxis(a, dim, 0) for a, dim in zip(arrays, dims)]
    both = jnp.concatenate([t.reshape(len(t), -1) for t in turned], axis=1)
    out, at, finished = (lax.all_gather(both, axis, axis=0, tiled=True), 0, [])
    for t, dim in zip(turned, dims):
        piece = out[:, at : at + t[0].size].reshape(-1, *t.shape[1:])
        finished.append(jnp.moveaxis(piece, 0, dim))
        at += t[0].size
    return tuple(finished)


def neutral_like(x, identity):
    return jax.tree.map(
        lambda a, e: jnp.broadcast_to(jnp.asarray(e, a.dtype), a.shape), x, identity
    )


def entering(x, axes, combine, identity):
    before = start = neutral_like(x, identity)
    subtotal = x
    for axis in reversed(axes):
        length, position = (lax.axis_size(axis), lax.axis_index(axis))
        pieces = jax.tree.map(
            lambda part, kind: lax.all_gather(part.astype(kind), axis),
            subtotal,
            (jnp.bfloat16, jnp.bfloat16),
        )
        inside, subtotal = (start, start)
        for k in range(length):
            passed = k < position
            subtotal = combine(
                subtotal, jax.tree.map(lambda part, own: part[k].astype(own.dtype), pieces, x)
            )
            inside = jax.tree.map(lambda new, old: jnp.where(passed, new, old), subtotal, inside)
        before = combine(inside, before)
    return before


def passed_along(x, axis, by):
    length = lax.axis_size(axis)
    pairs = [(i, i + by) for i in range(length) if 0 <= i + by < length]
    return lax.ppermute(x, axis, pairs)


def rotate(vectors, positions):
    head_width = vectors.shape[-1]
    half_width = head_width // 2
    inverse_freq = rope_base ** (-2.0 * jnp.arange(half_width, dtype=jnp.float32) / head_width)
    angles = positions[:, None] * inverse_freq[None, :]
    cosine = jnp.cos(angles)[:, None, :]
    sine_part = jnp.sin(angles)[:, None, :]
    front = vectors[..., :half_width]
    second = vectors[..., half_width:]
    return jnp.concatenate(
        [front * cosine - second * sine_part, front * sine_part + second * cosine], axis=-1
    )


def layer_norm(values, gain, shift):
    average = values.mean(-1, keepdims=True)
    spread = jnp.square(values - average).mean(-1, keepdims=True)
    return (values - average) * lax.rsqrt(spread + tiny_stabilizer) * gain + shift


def block_parts(query_tile, lookup_piece, payload_piece, log_blk):
    cum_log = jnp.cumsum(log_blk, axis=0)
    cum_heads = cum_log.T
    log_gap = cum_heads[:, :, None] - cum_heads[:, None, :]
    offsets = jnp.arange(log_blk.shape[0])
    causal = (offsets[:, None] >= offsets[None, :])[None]
    weight = jnp.where(causal, jnp.exp(jnp.where(causal, log_gap, 0.0)), 0.0)
    score_matrix = jnp.einsum(
        "jka,ska->kjs", query_tile, lookup_piece, preferred_element_type=jnp.float32
    )
    segment_scaling = (score_matrix * weight).astype(jnp.bfloat16)
    within = jnp.einsum(
        "htm,mhe->the", segment_scaling, payload_piece, preferred_element_type=jnp.float32
    )
    block_total = cum_log[-1]
    to_end = jnp.exp(block_total[None, :] - cum_log)
    faded_lookup_vector = (lookup_piece.astype(jnp.float32) * to_end[:, :, None]).astype(
        jnp.bfloat16
    )
    summand_term = jnp.einsum(
        "ajo,ajd->jod", faded_lookup_vector, payload_piece, preferred_element_type=jnp.float32
    )
    scaled_query = (query_tile.astype(jnp.float32) * jnp.exp(cum_log)[:, :, None]).astype(
        jnp.bfloat16
    )
    return (within, scaled_query, summand_term, jnp.exp(block_total))


def causal_conv(rows, edge_rows, taps, shift):
    padded = jnp.concatenate([edge_rows, rows], axis=0).astype(jnp.float32)
    length = rows.shape[0]
    result = shift[None, :] + padded[0:length] * taps[0]
    result = result + padded[1 : length + 1] * taps[1]
    return result + padded[2 : length + 2] * taps[2]


def combine(earlier, later):
    return (earlier[0] * later[0], later[0][:, None, None] * earlier[1] + later[1])


def shards(
    query_proj,
    key_proj,
    value_proj,
    gate_proj,
    log_decay,
    residual,
    out_weight,
    norm_gain,
    norm_bias,
    up_gate,
    up_value,
    conv_weight,
    conv_bias,
    down_weight,
):
    tok_rows = query_proj.shape[0]
    head_count = log_decay.shape[1]
    key_width = query_proj.shape[1] // head_count
    value_width = value_proj.shape[1] // head_count
    full_gate, full_value, full_down = turned_gather(
        (up_gate, up_value, down_weight), SP, (0, 0, 1)
    )
    positions = (lax.axis_index(SP) * tok_rows + jnp.arange(tok_rows)).astype(jnp.float32)
    query_rot = rotate(
        query_proj.astype(jnp.float32).reshape(tok_rows, head_count, key_width), positions
    ).astype(jnp.bfloat16)
    key_rot = (
        rotate(key_proj.astype(jnp.float32).reshape(tok_rows, head_count, key_width), positions)
        * key_width ** (-0.5)
    ).astype(jnp.bfloat16)
    block_count = tok_rows // BLOCK
    asking_segments = query_rot.reshape(block_count, BLOCK, head_count, key_width)
    key_blocks = key_rot.reshape(block_count, BLOCK, head_count, key_width)
    value_blocks = value_proj.reshape(block_count, BLOCK, head_count, value_width)
    log_blocks = log_decay.reshape(block_count, BLOCK, head_count)
    within, scaled_query, summand_term, block_decay = jax.vmap(block_parts)(
        asking_segments, key_blocks, value_blocks, log_blocks
    )

    def absorb(carry_state, pieces):
        return (pieces[1][:, None, None] * carry_state + pieces[0], None)

    zero_state = jnp.zeros((head_count, key_width, value_width), jnp.float32)
    own_state, _ = lax.scan(absorb, zero_state, (summand_term, block_decay))
    own_decay = jnp.prod(block_decay, axis=0)
    _, incoming = entering(
        (own_decay, own_state), SP, combine, (jnp.ones_like(own_decay), zero_state)
    )

    def advance(carry_state, pieces):
        carried = jnp.einsum(
            "thd,hde->the",
            pieces[0],
            carry_state.astype(jnp.bfloat16),
            preferred_element_type=jnp.float32,
        )
        return (pieces[2][:, None, None] * carry_state + pieces[1], carried)

    _, carried = lax.scan(advance, incoming, (scaled_query, summand_term, block_decay))
    mixed_heads = (within + carried).reshape(tok_rows, head_count, value_width)
    average = mixed_heads.mean(-1, keepdims=True)
    spread = jnp.square(mixed_heads - average).mean(-1, keepdims=True)
    standardized_rows = (mixed_heads - average) * lax.rsqrt(spread + tiny_stabilizer)
    gate_heads = gate_proj.astype(jnp.float32).reshape(tok_rows, head_count, value_width)
    gated_rows = (
        (jax.nn.silu(gate_heads) * standardized_rows)
        .astype(jnp.bfloat16)
        .reshape(tok_rows, head_count * value_width)
    )
    own_count = tok_rows // lax.axis_size("tp")
    partial_rows = jnp.dot(gated_rows, out_weight, preferred_element_type=jnp.float32)
    attended = lax.psum(partial_rows.astype(jnp.bfloat16), "tp").astype(jnp.float32)
    whole_rows = layer_norm(
        alpha_scale * residual.astype(jnp.float32) + attended, norm_gain[0], norm_bias[0]
    ).astype(jnp.bfloat16)
    normed_own = lax.dynamic_slice_in_dim(
        whole_rows, lax.axis_index("tp") * own_count, own_count, 0
    )
    gate_up = jnp.dot(whole_rows, full_gate, preferred_element_type=jnp.float32)
    value_up = jnp.dot(whole_rows, full_value, preferred_element_type=jnp.float32)
    gate_up = gate_up.astype(jnp.bfloat16)
    value_up = value_up.astype(jnp.bfloat16)
    gate_edge, value_edge = passed_along((gate_up[tok_rows - 2 :], value_up[tok_rows - 2 :]), SP, 1)
    gate_conv = causal_conv(gate_up, gate_edge, conv_weight[0], conv_bias[0])
    value_conv = causal_conv(value_up, value_edge, conv_weight[1], conv_bias[1])
    activated = (jax.nn.gelu(gate_conv) * value_conv).astype(jnp.bfloat16)
    partial_ffn = jnp.dot(activated, full_down, preferred_element_type=jnp.float32)
    ffn_out = lax.psum_scatter(
        partial_ffn.astype(jnp.bfloat16), "tp", scatter_dimension=0, tiled=True
    ).astype(jnp.float32)
    return layer_norm(
        alpha_scale * normed_own.astype(jnp.float32) + ffn_out, norm_gain[1], norm_bias[1]
    ).astype(jnp.bfloat16)


def solution(mesh):
    torus = Mesh(mesh.devices.reshape(4, 4, mesh.shape["tp"]), ("sp_0", "sp_1", "tp"))
    return jax.shard_map(
        shards,
        mesh=torus,
        in_specs=(
            P(SP, "tp"),
            P(SP, "tp"),
            P(SP, "tp"),
            P(SP, "tp"),
            P(SP, "tp"),
            P(SP, None),
            P("tp", None),
            P(),
            P(),
            P(SP, "tp"),
            P(SP, "tp"),
            P(None, None, "tp"),
            P(None, "tp"),
            P("tp", SP),
        ),
        out_specs=P(SP_TP, None),
        check_vma=False,
    )
```

profile of v0, /device:TPU:0, one launch (start us, length us, event | category | flops | bytes accessed | tf_op | source)
XLA Modules:
  0.0 287.6 jit_solution(7384815758810816143)
XLA Ops:
  7.4 2.4 reduce-window.6
  10.4 1.4 bitcast_convert_fusion
  11.8 3.1 %fusion.56 = (bf16[1024,1,128]{2,0,1:T(8,128)(2,1)S(1)}, bf16[1024,1,128]{2,0,1:T(8,128)(2,1)}, f32[1024,1,128]{2,0,1:T(8,128)S(1)}, f32[1024,1,128]{2,0,1:T(8,128)S(1)}) fusion(f32[1024,1,256]{2,0,1:T(8,128)S(1)} %get-tuple-element.170, f32[128]{0:T(128)S(1)} %multiply_power_fusion, f32[1024]{0:T(1024)S(1)} %add_convert_fusion.2, ...), kind=kLoop, calls=%fused_computation.87 | loop fusion | flops 1966080 | bytes 3674624 | tf_op jit(solution)/shard_map/convert.17
  14.9 0.8 copy-done.5
  15.7 2.0 convolution_bitcast_fusion.1
  17.7 9.8 %while.24 = (s32[]{:T(128)}, f32[1,256,512]{2,1,0:T(8,128)S(1)}, f32[4,1]{0,1:T(1,128)S(1)}, f32[4,1,256,512]{3,2,1,0:T(8,128)}, s32[]{:T(128)}, /*index=5*/s32[]{:T(128)}) while((s32[]{:T(128)}, f32[1,256,512]{2,1,0:T(8,128)S(1)}, f32[4,1]{0,1:T(1,128)S(1)}, f32[4,1,256,512]{3,2,1,0:T(8,128)}, s32[]{:T(128)}, ...), condition=%wide.region_4.5_spmd.clone, body=%wide.region_3.4_spmd.clone.sunk | while | flops 393219 | bytes 1572971 | solution.py:165
  18.3 1.8 bitcast_add_fusion.8
  20.2 0.6 constant_dynamic-slice_fusion.5
  20.8 1.8 bitcast_add_fusion.8
  22.6 0.6 constant_dynamic-slice_fusion.5
  23.2 1.8 bitcast_add_fusion.8
  25.7 1.8 bitcast_add_fusion.8
  27.5 0.7 convert_element_type.303
  28.3 0.7 dynamic-slice
  29.0 0.7 exponential_reduce_fusion
  29.7 1.4 dynamic-update-slice
  31.0 10.8 %all-reduce = bf16[4]{0:T(256)(128)(2,1)S(1)} all-reduce(bf16[4]{0:T(256)(128)(2,1)S(1)} %dynamic-update-slice), channel_id=1, replica_groups=mesh['sp_0'=4,'sp_1'=4,'tp'=8] {'sp_1'}, use_global_device_ids=true, to_apply=%add | all-reduce | flops 4 | bytes 16
  41.9 0.7 slice_convert_fusion.3
  43.2 11.9 %all-gather.10.cloned.1.call-done = bf16[4,256,512]{2,1,0:T(8,128)(2,1)} async-done(((bf16[1,256,512]{2,1,0:T(8,128)(2,1)}), bf16[4,256,512]{2,1,0:T(8,128)(2,1)}) %all-gather.10.cloned.1.call-update) | async-done | bytes 1048592 | tf_op jit(solution)/shard_map/all_gather | solution.py:40
  55.0 4.0 %fusion.70 = bf16[1,1,256,512]{3,2,1,0:T(8,128)(2,1)} fusion(f32[]{:T(128)} %bitcast.39, f32[]{:T(128)} %bitcast.40, f32[]{:T(128)} %bitcast.41, f32[]{:T(128)} %bitcast.42, bf16[4,256,512]{2,1,0:T(8,128)(2,1)} %all-gather.10.cloned.1.call-done), kind=kLoop, calls=%fused_computation.102 | loop fusion | flops 1572864 | bytes 1310736 | tf_op jit(solution)/shard_map/convert_element_type | solution.py:40
  59.1 0.7 dynamic-slice.1
  59.7 0.6 fusion.100
  60.4 1.4 dynamic-update-slice.1
  61.8 10.7 %all-reduce.1 = bf16[4]{0:T(256)(128)(2,1)S(1)} all-reduce(bf16[4]{0:T(256)(128)(2,1)S(1)} %dynamic-update-slice.1), channel_id=2, replica_groups=mesh['sp_0'=4,'sp_1'=4,'tp'=8] {'sp_0'}, use_global_device_ids=true, to_apply=%add.1 | all-reduce | flops 4 | bytes 16
  72.5 0.7 fusion.99
  78.2 1.9 fusion.61
  80.2 3.6 %all-gather.6.cloned.1.call-done = bf16[4,1,256,512]{3,2,1,0:T(8,128)(2,1)} async-done(((bf16[1,1,256,512]{3,2,1,0:T(8,128)(2,1)}), bf16[4,1,256,512]{3,2,1,0:T(8,128)(2,1)}) %all-gather.6.cloned.1.call-update) | async-done | bytes 1048592 | tf_op jit(solution)/shard_map/all_gather | solution.py:40
  83.8 3.9 %fusion.69 = f32[1,256,512]{2,1,0:T(8,128)S(1)} fusion(bf16[4,1,256,512]{3,2,1,0:T(8,128)(2,1)} %all-gather.6.cloned.1.call-done, f32[]{:T(128)} %bitcast.39, f32[]{:T(128)} %bitcast.40, f32[]{:T(128)} %bitcast.41, f32[]{:T(128)} %bitcast.42, f32[]{:T(128)} %bitcast.33, f32[]{:T(128)S(6)} %convert.26, f32[]{:T(128)S(6)} %convert.27, f32[]{:T(128)} %bitcast.38, ...), kind=kLoop, calls=%fused_computation.99 | loop fusion | flops 4194304 | bytes 2621484 | tf_op jit(solution)/shard_map/add | solution.py:118
  87.7 17.8 %while.23 = (s32[]{:T(128)}, f32[1,256,512]{2,1,0:T(8,128)S(1)}, f32[4,256,1,512]{3,1,2,0:T(8,128)}, f32[4,1]{0,1:T(1,128)S(1)}, f32[4,1,256,512]{3,2,1,0:T(8,128)}, /*index=5*/bf16[4,256,1,256]{3,1,2,0:T(8,128)(2,1)}, s32[]{:T(128)}) while((s32[]{:T(128)}, f32[1,256,512]{2,1,0:T(8,128)S(1)}, f32[4,256,1,512]{3,1,2,0:T(8,128)}, ...), condition=%wide.region_6.7_spmd, body=%wide.region_5.6_spmd.sunk | while | flops 67502080 | bytes 2753641 | solution.py:180
  87.7 0.6 constant_dynamic-slice_fusion.4
  88.4 1.9 fusion.117
  90.3 1.9 bitcast_add_fusion.7
  92.2 0.6 constant_dynamic-slice_fusion.4
  92.8 1.9 fusion.117
  94.7 1.9 bitcast_add_fusion.7
  96.6 0.6 constant_dynamic-slice_fusion.4
  97.2 1.9 fusion.117
  99.2 1.9 bitcast_add_fusion.7
  101.1 0.6 constant_dynamic-slice_fusion.4
  101.7 1.9 fusion.117
  103.6 1.9 bitcast_add_fusion.7
  105.5 4.2 %fusion.101 = (f32[4,256]{1,0:T(4,128)S(1)}, f32[4,256,1,512]{3,1,0,2:T(8,128)}) fusion(f32[4,256,1,512]{3,1,2,0:T(8,128)} %get-tuple-element.60, bf16[4,256,512]{2,1,0:T(8,128)(2,1)} %bitcast.150, bf16[4,256,128]{2,1,0:T(8,128)(2,1)} %bitcast.155, bf16[4,256,128]{2,1,0:T(8,128)(2,1)S(1)} %bitcast.153, f32[4,256]{1,0:T(4,128)S(1)} %get-tuple-element.135, ...), kind=kOutput, calls=%fused_computation.158 | convolution fusion | flops 406846464 | bytes 6889472 | tf_op jit(solution)/shard_map/vmap(htm,mhe->the)/dot_general | solution.py:92
  109.8 2.1 multiply_reduce_fusion.1
  112.0 2.2 fusion.32
  114.2 4.3 %convolution_convert_fusion.1 = bf16[1024,2048]{1,0:T(8,128)(2,1)} fusion(bf16[1024,512]{1,0:T(8,128)(2,1)S(1)} %fusion.32, bf16[512,2048]{1,0:T(8,128)(2,1)S(1)} %copy-done), kind=kOutput, calls=%fused_computation.18 | convolution fusion | flops 2149580800 | bytes 7340032 | tf_op jit(solution)/shard_map/dot_general | solution.py:192
  118.6 0.8 copy-done.7
  119.5 0.8 pad_maximum_fusion
  120.8 71.2 %all-reduce.4.cloned.1.call-done = bf16[1024,2048]{1,0:T(8,128)(2,1)} async-done(((bf16[1024,2048]{1,0:T(8,128)(2,1)}), bf16[1024,2048]{1,0:T(8,128)(2,1)}) %all-reduce.4.cloned.1.call-update) | async-done | bytes 4194320 | tf_op jit(solution)/shard_map/psum | solution.py:193
  192.0 5.1 %fusion.6 = f32[1024]{0:T(1024)S(1)} fusion(bf16[1024,2048]{1,0:T(8,128)(2,1)} %all-reduce.4.cloned.1.call-done, bf16[1024,2048]{1,0:T(8,128)(2,1)} %param.23), kind=kLoop, calls=%fused_computation.15 | loop fusion | flops 10484736 | bytes 8392704 | tf_op jit(solution)/shard_map/reduce_sum | solution.py:76
  197.1 0.9 copy-done.2
  197.9 2.4 multiply_reduce_fusion
  200.4 4.0 %add_convert_fusion = bf16[1024,2048]{1,0:T(8,128)(2,1)} fusion(bf16[1024,2048]{1,0:T(8,128)(2,1)S(1)} %copy-done.2, bf16[1024,2048]{1,0:T(8,128)(2,1)S(1)} %copy-done.1, f32[2048]{0:T(1024)S(1)} %bitcast.164, f32[2048]{0:T(1024)S(1)} %bitcast.163, f32[1024]{0:T(1024)S(1)} %add_rsqrt_fusion, f32[1024]{0:T(1024)S(1)} %broadcast_multiply_fusion), kind=kLoop, calls=%fused_computation.12 | loop fusion | flops 18874368 | bytes 12607488 | tf_op jit(solution)/shard_map/convert_element_type | solution.py:196
  204.4 6.4 %fusion.33 = bf16[1024,704]{0,1:T(8,128)(2,1)S(1)} fusion(bf16[1024,2048]{1,0:T(8,128)(2,1)} %add_convert_fusion, bf16[2048,2112]{0,1:T(8,128)(2,1)} %all-gather.8.cloned.1.call-done), kind=kOutput, calls=%fused_computation.56 | convolution fusion | flops 2953510912 | bytes 8519680 | tf_op jit(solution)/shard_map/dot_general | solution.py:200
  210.9 3.3 %collective-permute-start = (bf16[2,704]{0,1:T(8,128)(2,1)S(1)}, bf16[2,704]{0,1:T(8,128)(2,1)S(1)}, u32[]{:S(2)}, u32[]{:S(2)}) collective-permute-start(bf16[2,704]{0,1:T(8,128)(2,1)S(1)} %slice.226), channel_id=1, source_target_pairs={{0,8},{8,16},{16,24},{24,32},{32,40},{40,48},{48,56},{56,64},{64,7... | collective-permute-start | bytes 8456 | tf_op jit(solution)/shard_map/ppermute | solution.py:58
  214.3 5.0 %fusion.36 = bf16[1024,704]{0,1:T(8,128)(2,1)S(1)} fusion(bf16[1024,2048]{1,0:T(8,128)(2,1)S(1)} %copy-done.4, bf16[2048,2112]{0,1:T(8,128)(2,1)} %all-gather.8.cloned.1.call-done), kind=kOutput, calls=%fused_computation.57 | convolution fusion | flops 2953510912 | bytes 8519680 | tf_op jit(solution)/shard_map/dot_general | solution.py:201
  219.4 3.6 %collective-permute-start.1 = (bf16[2,704]{0,1:T(8,128)(2,1)S(1)}, bf16[2,704]{0,1:T(8,128)(2,1)S(1)}, u32[]{:S(2)}, u32[]{:S(2)}) collective-permute-start(bf16[2,704]{0,1:T(8,128)(2,1)S(1)} %slice.231), channel_id=1, source_target_pairs={{0,8},{8,16},{16,24},{24,32},{32,40},{40,48},{48,56},{56,64},{64,7... | collective-permute-start | bytes 8456 | tf_op jit(solution)/shard_map/ppermute | solution.py:58
  223.1 0.8 maximum_convert_fusion
  223.8 2.0 collective-permute-done.1
  225.8 0.8 maximum_convert_fusion.1
  226.6 10.0 %convolution_convert_fusion = bf16[1024,2048]{1,0:T(8,128)(2,1)} fusion(bf16[2048,2112]{0,1:T(8,128)(2,1)} %all-gather.8.cloned.1.call-done, f32[1026,704]{0,1:T(8,128)S(1)} %maximum_convert_fusion.1, f32[1026,704]{0,1:T(8,128)S(1)} %maximum_convert_fusion, f32[704]{0:T(1024)S(1)} %get-tuple-element.110, f32[704]{0:T(1024)S(1)} %get-tuple-element.111, ...), kind=kOutput, calls=%fused_computation.17 | convolution fusion | flops 2970746880 | bytes 24412160 | tf_op jit(solution)/shard_map/dot_general | solution.py:208
  236.6 38.6 %reduce-scatter.2.cloned.1.call-done = bf16[128,2048]{1,0:T(8,128)(2,1)} async-done(((bf16[1024,2048]{1,0:T(8,128)(2,1)}), bf16[128,2048]{1,0:T(8,128)(2,1)}) %reduce-scatter.2.cloned.1.call-update) | async-done | bytes 524304 | tf_op jit(solution)/shard_map/reduce_scatter | solution.py:209
  275.2 1.5 fusion.46
  276.7 1.5 multiply_reduce_fusion.2
  278.2 2.3 add_convert_fusion.1
  (74 shorter events, 2.9 us)
Async XLA Ops:
  7.4 106.8 %copy-start = (bf16[512,2048]{1,0:T(8,128)(2,1)S(1)}, bf16[512,2048]{1,0:T(8,128)(2,1)}, u32[]{:S(2)}) copy-start(bf16[512,2048]{1,0:T(8,128)(2,1)} %param.24) | copy-start | bytes 6291460
  7.4 47.7 %all-gather.10.cloned.1.call-start = ((), (), s32[]{:S(2)}) async-start(), calls=%async_computation.5 | async-start | bytes 1310720 | tf_op jit(solution)/shard_map/all_gather | solution.py:40
  10.4 5.3 %copy-start.6 = (bf16[1024,512]{1,0:T(8,128)(2,1)S(1)}, bf16[1024,512]{1,0:T(8,128)(2,1)}, u32[]{:S(2)}) copy-start(bf16[1024,512]{1,0:T(8,128)(2,1)} %param.20) | copy-start | bytes 3145732
  14.9 0.8 copy-start.5
  17.7 10.6 %copy-start.15 = (u32[128]{0:T(128)S(1)}, u32[128]{0:T(128)}, u32[]{:S(2)}) copy-start(u32[128]{0:T(128)} %constant.102) | copy-start | bytes 1540
  17.7 41.3 %copy-start.14 = (u32[128]{0:T(128)S(1)}, u32[128]{0:T(128)}, u32[]{:S(2)}) copy-start(u32[128]{0:T(128)} %constant.107) | copy-start | bytes 1540
  28.3 55.6 %all-gather.6.cloned.1.call-start = ((), (), s32[]{:S(2)}) async-start(), calls=%async_computation.1 | async-start | bytes 1310720 | tf_op jit(solution)/shard_map/all_gather | solution.py:40
  59.0 133.0 %all-reduce.4.cloned.1.call-start = ((), (), s32[]{:S(2)}) async-start(), calls=%async_computation.2 | async-start | bytes 8388608 | tf_op jit(solution)/shard_map/psum | solution.py:193
  109.7 2.2 copy-start.3
  118.4 0.9 copy-start.7
  118.5 1.0 copy-start.8
  118.5 1.1 copy-start.9
  118.5 2.2 copy-start.13
  118.5 2.2 copy-start.10
  118.5 2.3 copy-start.11
  118.5 2.3 copy-start.12
  118.5 85.9 %all-gather.8.cloned.1.call-start = ((), (), s32[]{:S(2)}) async-start(), calls=%async_computation.3 | async-start | bytes 9191424 | tf_op jit(solution)/shard_map/all_gather | solution.py:20
  120.4 154.8 %reduce-scatter.2.cloned.1.call-start = ((), (), s32[]{:S(2)}) async-start(), calls=%async_computation.4 | async-start | bytes 4718592 | tf_op jit(solution)/shard_map/reduce_scatter | solution.py:209
  192.0 5.1 %copy-start.1 = (bf16[1024,2048]{1,0:T(8,128)(2,1)S(1)}, bf16[1024,2048]{1,0:T(8,128)(2,1)}, u32[]{:S(2)}) copy-start(bf16[1024,2048]{1,0:T(8,128)(2,1)} %param.23) | copy-start | bytes 12582916
  192.0 6.0 %copy-start.2 = (bf16[1024,2048]{1,0:T(8,128)(2,1)S(1)}, bf16[1024,2048]{1,0:T(8,128)(2,1)}, u32[]{:S(2)}) copy-start(bf16[1024,2048]{1,0:T(8,128)(2,1)} %all-reduce.4.cloned.1.call-done) | copy-start | bytes 12582916
  204.4 9.9 %copy-start.4 = (bf16[1024,2048]{1,0:T(8,128)(2,1)S(1)}, bf16[1024,2048]{1,0:T(8,128)(2,1)}, u32[]{:S(2)}) copy-start(bf16[1024,2048]{1,0:T(8,128)(2,1)} %add_convert_fusion) | copy-start | bytes 12582916
  210.9 12.1 %collective-permute-start = (bf16[2,704]{0,1:T(8,128)(2,1)S(1)}, bf16[2,704]{0,1:T(8,128)(2,1)S(1)}, u32[]{:S(2)}, u32[]{:S(2)}) collective-permute-start(bf16[2,704]{0,1:T(8,128)(2,1)S(1)} %slice.226), channel_id=1, source_target_pairs={{0,8},{8,16},{16,24},{24,32},{32,40},{40,48},{48,56},{56,64},{64,7... | collective-permute-start | bytes 8456 | tf_op jit(solution)/shard_map/ppermute | solution.py:58
  219.4 6.4 %collective-permute-start.1 = (bf16[2,704]{0,1:T(8,128)(2,1)S(1)}, bf16[2,704]{0,1:T(8,128)(2,1)S(1)}, u32[]{:S(2)}, u32[]{:S(2)}) collective-permute-start(bf16[2,704]{0,1:T(8,128)(2,1)S(1)} %slice.231), channel_id=1, source_target_pairs={{0,8},{8,16},{16,24},{24,32},{32,40},{40,48},{48,56},{56,64},{64,7... | collective-permute-start | bytes 8456 | tf_op jit(solution)/shard_map/ppermute | solution.py:58
Sparse Core Ops, SparseCore 0:
  28.4 26.5 all-gather.9
  59.1 24.6 all-gather.5
  118.6 73.2 all-reduce.3
  236.7 38.4 reduce-scatter.1
Sparse Core Ops, SparseCore 1:
  121.1 78.5 all-gather.7
where the time goes:
time: 289 us; the launch traced here: 288 us
  waiting for transfers between devices  127 us (44%)
  other arithmetic  58 us (20%)
  matrix products  39.6 us (14%)
  blocking collectives  21.5 us (7%)
  between operations  20.6 us (7%)
  local copies, waits for them, and re-layouts  13.1 us (5%)
  starting transfers between devices  7.31 us (3%)
    psum x1, waiting for transfers between devices, shards(): lax.psum(partial_rows.astype(jnp.bfloat16), 'tp').astype(jnp.float32)  71.2 us
    reduce_scatter x1, waiting for transfers between devices, shards(): lax.psum_scatter(partial_ffn.astype(jnp.bfloat16), 'tp', scatter_dimensio...  38.6 us
    unnamed x2, blocking collectives  21.5 us
    all_gather x2, waiting for transfers between devices, entering(): lax.all_gather(part.astype(kind), axis)  15.5 us
    dot_general x1, matrix products, shards(): jnp.dot(activated, full_down, preferred_element_type=jnp.float32)  9.97 us
    dot_general x4, matrix products, advance(): jnp.einsum('thd,hde->the', pieces[0], carry_state.astype(jnp.bfloat16), p...  7.74 us
    add x4, other arithmetic, advance(): return (pieces[2][:, None, None] * carry_state + pieces[1], carried)  7.52 us
    add x4, other arithmetic, absorb(): return (pieces[1][:, None, None] * carry_state + pieces[0], None)  7.35 us
  transfers between devices with their start and end apart: 7, of which 5 were waited for; matrix products, arithmetic and copies ran while one was open for 9% of the time, Pallas kernels for 0%

commit v1 on v0

--- a/solution.py
+++ b/solution.py
@@ -190,18 +190,23 @@
     )
     own_count = tok_rows // lax.axis_size("tp")
     partial_rows = jnp.dot(gated_rows, out_weight, preferred_element_type=jnp.float32)
-    attended = lax.psum(partial_rows.astype(jnp.bfloat16), "tp").astype(jnp.float32)
-    whole_rows = layer_norm(
-        alpha_scale * residual.astype(jnp.float32) + attended, norm_gain[0], norm_bias[0]
-    ).astype(jnp.bfloat16)
-    normed_own = lax.dynamic_slice_in_dim(
-        whole_rows, lax.axis_index("tp") * own_count, own_count, 0
-    )
+    attended = lax.psum_scatter(
+        partial_rows.astype(jnp.bfloat16), "tp", scatter_dimension=0, tiled=True
+    ).astype(jnp.float32)
+    own_residual = lax.dynamic_slice_in_dim(
+        residual, lax.axis_index("tp") * own_count, own_count, 0
+    )
+    normed_own = layer_norm(
+        alpha_scale * own_residual.astype(jnp.float32) + attended, norm_gain[0], norm_bias[0]
+    ).astype(jnp.bfloat16)
+    whole_rows = lax.all_gather(normed_own, "tp", axis=0, tiled=True)
     gate_up = jnp.dot(whole_rows, full_gate, preferred_element_type=jnp.float32)
     value_up = jnp.dot(whole_rows, full_value, preferred_element_type=jnp.float32)
     gate_up = gate_up.astype(jnp.bfloat16)
     value_up = value_up.astype(jnp.bfloat16)
-    gate_edge, value_edge = passed_along((gate_up[tok_rows - 2 :], value_up[tok_rows - 2 :]), SP, 1)
+    edges = jnp.concatenate([gate_up[tok_rows - 2 :], value_up[tok_rows - 2 :]], axis=0)
+    edges = passed_along(edges, SP, 1)
+    gate_edge, value_edge = edges[:2], edges[2:]
     gate_conv = causal_conv(gate_up, gate_edge, conv_weight[0], conv_bias[0])
     value_conv = causal_conv(value_up, value_edge, conv_weight[1], conv_bias[1])
     activated = (jax.nn.gelu(gate_conv) * value_conv).astype(jnp.bfloat16)

time: 289 us -> 316 us (1.093)
  waiting for transfers between devices: 127 us -> 165 us
  other arithmetic: 58 us -> 51.6 us
  starting transfers between devices: 7.31 us -> 4.01 us
    psum x1 -> x0, waiting for transfers between devices: 71.2 us -> none  [shards(): lax.psum(partial_rows.astype(jnp.bfloat16), 'tp').astype(jnp.float32)]
    reduce_scatter x0 -> x1, waiting for transfers between devices: none -> 36.8 us  [shards(): lax.psum_scatter(partial_rows.astype(jnp.bfloat16), 'tp', scatter_dimensi...]
    all_gather x1, waiting for transfers between devices: 0.01 us -> 36.6 us  [turned_gather(): out, at, finished = (lax.all_gather(both, axis, axis=0, tiled=True), 0, [])]
    all_gather x0 -> x1, waiting for transfers between devices: none -> 32.7 us  [shards(): whole_rows = lax.all_gather(normed_own, 'tp', axis=0, tiled=True)]
    reduce_sum x2, other arithmetic: 6.53 us -> 2.79 us  [layer_norm(): average = values.mean(-1, keepdims=True)]
    ppermute x2 -> x1, starting transfers between devices: 6.96 us -> 3.62 us  [passed_along(): return lax.ppermute(x, axis, pairs)]
    unnamed x40 -> x38, local copies, waits for them, and re-layouts: 6.91 us -> 6.06 us
  transfers between devices with their start and end apart: 7 -> 7, of which waited for: 5 -> 7; matrix products, arithmetic and copies ran while one was open for 9% -> 5% of each run, Pallas kernels for 0% -> 0%
where the time goes in v1:
time: 316 us; the launch traced here: 314 us
  waiting for transfers between devices  165 us (52%)
  other arithmetic  51.6 us (16%)
  matrix products  39.7 us (13%)
  blocking collectives  21.5 us (7%)
  between operations  20.6 us (7%)
  local copies, waits for them, and re-layouts  12.4 us (4%)
  starting transfers between devices  4.01 us (1%)
    reduce_scatter x1, waiting for transfers between devices, shards(): lax.psum_scatter(partial_ffn.astype(jnp.bfloat16), 'tp', scatter_dimensio...  38.9 us
    reduce_scatter x1, waiting for transfers between devices, shards(): lax.psum_scatter(partial_rows.astype(jnp.bfloat16), 'tp', scatter_dimensi...  36.8 us
    all_gather x1, waiting for transfers between devices, turned_gather(): out, at, finished = (lax.all_gather(both, axis, axis=0, tiled=True), 0, [])  36.6 us
    all_gather x1, waiting for transfers between devices, shards(): whole_rows = lax.all_gather(normed_own, 'tp', axis=0, tiled=True)  32.7 us
    unnamed x2, blocking collectives  21.5 us
    all_gather x2, waiting for transfers between devices, entering(): lax.all_gather(part.astype(kind), axis)  15.5 us
    dot_general x1, matrix products, shards(): jnp.dot(activated, full_down, preferred_element_type=jnp.float32)  10 us
    dot_general x4, matrix products, advance(): jnp.einsum('thd,hde->the', pieces[0], carry_state.astype(jnp.bfloat16), p...  7.74 us
  transfers between devices with their start and end apart: 7, of which 7 were waited for; matrix products, arithmetic and copies ran while one was open for 5% of the time, Pallas kernels for 0%

profile of v1, /device:TPU:0, one launch (start us, length us, event | category | flops | bytes accessed | tf_op | source)
XLA Modules:
  0.0 314.5 jit_solution(11302256274251141249)
XLA Ops:
  7.4 2.4 reduce-window.6
  10.4 1.4 bitcast_convert_fusion
  11.8 3.1 fusion.56
  14.9 0.8 copy-done.3
  15.7 2.0 convolution_bitcast_fusion.1
  17.7 9.8 %while.24 = (s32[]{:T(128)}, f32[1,256,512]{2,1,0:T(8,128)S(1)}, f32[4,1]{0,1:T(1,128)S(1)}, f32[4,1,256,512]{3,2,1,0:T(8,128)}, s32[]{:T(128)}, /*index=5*/s32[]{:T(128)}) while((s32[]{:T(128)}, f32[1,256,512]{2,1,0:T(8,128)S(1)}, f32[4,1]{0,1:T(1,128)S(1)}, f32[4,1,256,512]{3,2,1,0:T(8,128)}, s32[]{:T(128)}, ...), condition=%wide.region_4.5_spmd.clone, body=%wide.region_3.4_spmd.clone.sunk | while | flops 393219 | bytes 1572971 | solution.py:165
  18.3 1.8 bitcast_add_fusion.8
  20.2 0.6 constant_dynamic-slice_fusion.5
  20.8 1.8 bitcast_add_fusion.8
  22.6 0.6 constant_dynamic-slice_fusion.5
  23.2 1.8 bitcast_add_fusion.8
  25.7 1.8 bitcast_add_fusion.8
  27.5 0.7 convert_element_type.303
  28.3 0.7 dynamic-slice
  29.0 0.7 exponential_reduce_fusion
  29.7 1.4 dynamic-update-slice
  31.0 10.8 %all-reduce = bf16[4]{0:T(256)(128)(2,1)S(1)} all-reduce(bf16[4]{0:T(256)(128)(2,1)S(1)} %dynamic-update-slice), channel_id=1, replica_groups=mesh['sp_0'=4,'sp_1'=4,'tp'=8] {'sp_1'}, use_global_device_ids=true, to_apply=%add | all-reduce | flops 4 | bytes 16
  41.9 0.7 slice_convert_fusion.3
  43.2 11.9 %all-gather.13.cloned.1.call-done = bf16[4,256,512]{2,1,0:T(8,128)(2,1)} async-done(((bf16[1,256,512]{2,1,0:T(8,128)(2,1)}), bf16[4,256,512]{2,1,0:T(8,128)(2,1)}) %all-gather.13.cloned.1.call-update) | async-done | bytes 1048592 | tf_op jit(solution)/shard_map/all_gather | solution.py:40
  55.0 4.0 %fusion.70 = bf16[1,1,256,512]{3,2,1,0:T(8,128)(2,1)} fusion(f32[]{:T(128)} %bitcast.39, f32[]{:T(128)} %bitcast.40, f32[]{:T(128)} %bitcast.41, f32[]{:T(128)} %bitcast.42, bf16[4,256,512]{2,1,0:T(8,128)(2,1)} %all-gather.13.cloned.1.call-done), kind=kLoop, calls=%fused_computation.102 | loop fusion | flops 1572864 | bytes 1310736 | tf_op jit(solution)/shard_map/convert_element_type | solution.py:40
  59.1 0.7 dynamic-slice.1
  59.7 0.6 fusion.101
  60.4 1.4 dynamic-update-slice.1
  61.8 10.7 %all-reduce.1 = bf16[4]{0:T(256)(128)(2,1)S(1)} all-reduce(bf16[4]{0:T(256)(128)(2,1)S(1)} %dynamic-update-slice.1), channel_id=2, replica_groups=mesh['sp_0'=4,'sp_1'=4,'tp'=8] {'sp_0'}, use_global_device_ids=true, to_apply=%add.1 | all-reduce | flops 4 | bytes 16
  72.5 0.7 fusion.100
  78.2 1.9 fusion.61
  80.2 3.6 %all-gather.7.cloned.1.call-done = bf16[4,1,256,512]{3,2,1,0:T(8,128)(2,1)} async-done(((bf16[1,1,256,512]{3,2,1,0:T(8,128)(2,1)}), bf16[4,1,256,512]{3,2,1,0:T(8,128)(2,1)}) %all-gather.7.cloned.1.call-update) | async-done | bytes 1048592 | tf_op jit(solution)/shard_map/all_gather | solution.py:40
  83.8 3.9 %fusion.69 = f32[1,256,512]{2,1,0:T(8,128)S(1)} fusion(bf16[4,1,256,512]{3,2,1,0:T(8,128)(2,1)} %all-gather.7.cloned.1.call-done, f32[]{:T(128)} %bitcast.39, f32[]{:T(128)} %bitcast.40, f32[]{:T(128)} %bitcast.41, f32[]{:T(128)} %bitcast.42, f32[]{:T(128)} %bitcast.33, f32[]{:T(128)S(6)} %convert.26, f32[]{:T(128)S(6)} %convert.27, f32[]{:T(128)} %bitcast.38, ...), kind=kLoop, calls=%fused_computation.99 | loop fusion | flops 4194304 | bytes 2621484 | tf_op jit(solution)/shard_map/add | solution.py:118
  87.7 17.8 %while.23 = (s32[]{:T(128)}, f32[1,256,512]{2,1,0:T(8,128)S(1)}, f32[4,256,1,512]{3,1,2,0:T(8,128)}, f32[4,1]{0,1:T(1,128)S(1)}, f32[4,1,256,512]{3,2,1,0:T(8,128)}, /*index=5*/bf16[4,256,1,256]{3,1,2,0:T(8,128)(2,1)}, s32[]{:T(128)}) while((s32[]{:T(128)}, f32[1,256,512]{2,1,0:T(8,128)S(1)}, f32[4,256,1,512]{3,1,2,0:T(8,128)}, ...), condition=%wide.region_6.7_spmd, body=%wide.region_5.6_spmd.sunk | while | flops 67502080 | bytes 2753641 | solution.py:180
  87.7 0.6 constant_dynamic-slice_fusion.4
  88.4 1.9 fusion.118
  90.3 1.9 bitcast_add_fusion.7
  92.2 0.6 constant_dynamic-slice_fusion.4
  92.8 1.9 fusion.118
  94.7 1.9 bitcast_add_fusion.7
  96.6 0.6 constant_dynamic-slice_fusion.4
  97.2 1.9 fusion.118
  99.2 1.9 bitcast_add_fusion.7
  101.1 0.6 constant_dynamic-slice_fusion.4
  101.7 1.9 fusion.118
  103.6 1.9 bitcast_add_fusion.7
  105.5 4.2 %fusion.102 = (f32[4,256]{1,0:T(4,128)S(1)}, f32[4,256,1,512]{3,1,0,2:T(8,128)}) fusion(f32[4,256,1,512]{3,1,2,0:T(8,128)} %get-tuple-element.60, bf16[4,256,512]{2,1,0:T(8,128)(2,1)} %bitcast.150, bf16[4,256,128]{2,1,0:T(8,128)(2,1)} %bitcast.155, bf16[4,256,128]{2,1,0:T(8,128)(2,1)S(1)} %bitcast.153, f32[4,256]{1,0:T(4,128)S(1)} %get-tuple-element.145, ...), kind=kOutput, calls=%fused_computation.160 | convolution fusion | flops 406846464 | bytes 6889472 | tf_op jit(solution)/shard_map/vmap(htm,mhe->the)/dot_general | solution.py:92
  109.8 2.1 multiply_reduce_fusion
  112.0 2.2 fusion.31
  114.2 4.3 %convolution_convert_fusion.1 = bf16[1024,2048]{1,0:T(8,128)(2,1)} fusion(bf16[1024,512]{1,0:T(8,128)(2,1)S(1)} %fusion.31, bf16[512,2048]{1,0:T(8,128)(2,1)S(1)} %copy-done), kind=kOutput, calls=%fused_computation.14 | convolution fusion | flops 2149580800 | bytes 7340032 | tf_op jit(solution)/shard_map/dot_general | solution.py:192
  118.6 0.8 copy-done.5
  119.6 0.9 pad_maximum_fusion
  120.6 36.8 %reduce-scatter.3.cloned.1.call-done = bf16[128,2048]{1,0:T(8,128)(2,1)} async-done(((bf16[1024,2048]{1,0:T(8,128)(2,1)}), bf16[128,2048]{1,0:T(8,128)(2,1)}) %reduce-scatter.3.cloned.1.call-update) | async-done | bytes 524304 | tf_op jit(solution)/shard_map/reduce_scatter | solution.py:193
  157.4 1.5 fusion.45
  158.9 1.6 multiply_reduce_fusion.2
  160.4 2.4 add_convert_fusion.1
  163.1 36.6 %all-gather.11.cloned.1.call-done = bf16[2048,2112]{0,1:T(8,128)(2,1)} async-done(((bf16[128,2112]{0,1:T(8,128)(2,1)}), bf16[2048,2112]{0,1:T(8,128)(2,1)}) %all-gather.11.cloned.1.call-update) | async-done | bytes 8650768 | tf_op jit(solution)/shard_map/all_gather | solution.py:20
  199.7 32.7 %all-gather.9.cloned.1.call-done = bf16[1024,2048]{1,0:T(8,128)(2,1)} async-done(((bf16[128,2048]{1,0:T(8,128)(2,1)}), bf16[1024,2048]{1,0:T(8,128)(2,1)}) %all-gather.9.cloned.1.call-update) | async-done | bytes 4194320 | tf_op jit(solution)/shard_map/all_gather | solution.py:202
  232.4 6.4 %fusion.32 = bf16[1024,704]{0,1:T(8,128)(2,1)S(1)} fusion(bf16[1024,2048]{1,0:T(8,128)(2,1)} %all-gather.9.cloned.1.call-done, bf16[2048,2112]{0,1:T(8,128)(2,1)} %all-gather.11.cloned.1.call-done), kind=kOutput, calls=%fused_computation.52 | convolution fusion | flops 2953510912 | bytes 8519680 | tf_op jit(solution)/shard_map/dot_general | solution.py:203
  239.0 5.0 %fusion.35 = bf16[1024,704]{0,1:T(8,128)(2,1)S(1)} fusion(bf16[1024,2048]{1,0:T(8,128)(2,1)S(1)} %copy-done.12, bf16[2048,2112]{0,1:T(8,128)(2,1)} %all-gather.11.cloned.1.call-done), kind=kOutput, calls=%fused_computation.53 | convolution fusion | flops 2953510912 | bytes 8519680 | tf_op jit(solution)/shard_map/dot_general | solution.py:204
  244.3 3.6 %collective-permute-start = (bf16[4,704]{0,1:T(8,128)(2,1)S(1)}, bf16[4,704]{0,1:T(8,128)(2,1)S(1)}, u32[]{:S(2)}, u32[]{:S(2)}) collective-permute-start(bf16[4,704]{0,1:T(8,128)(2,1)S(1)} %pad_maximum_fusion.1), channel_id=1, source_target_pairs={{0,8},{8,16},{16,24},{24,32},{32,40},{40,48},{48,56},{56,64},{64,7... | collective-permute-start | bytes 16904 | tf_op jit(solution)/shard_map/ppermute | solution.py:58
  247.9 3.9 %collective-permute-done = bf16[4,704]{0,1:T(8,128)(2,1)S(1)} collective-permute-done((bf16[4,704]{0,1:T(8,128)(2,1)S(1)}, bf16[4,704]{0,1:T(8,128)(2,1)S(1)}, u32[]{:S(2)}, u32[]{:S(2)}) %collective-permute-start) | collective-permute-done | bytes 5664 | tf_op jit(solution)/shard_map/ppermute | solution.py:58
  252.0 0.8 maximum_convert_fusion
  252.8 0.8 maximum_convert_fusion.1
  253.5 10.0 %convolution_convert_fusion = bf16[1024,2048]{1,0:T(8,128)(2,1)} fusion(bf16[2048,2112]{0,1:T(8,128)(2,1)} %all-gather.11.cloned.1.call-done, f32[1026,704]{0,1:T(8,128)S(1)} %maximum_convert_fusion.1, f32[1026,704]{0,1:T(8,128)S(1)} %maximum_convert_fusion, f32[704]{0:T(1024)S(1)} %get-tuple-element.120, f32[704]{0:T(1024)S(1)} %get-tuple-element.121, ...), kind=kOutput, calls=%fused_computation.13 | convolution fusion | flops 2970746880 | bytes 24412160 | tf_op jit(solution)/shard_map/dot_general | solution.py:213
  263.6 38.9 %reduce-scatter.5.cloned.1.call-done = bf16[128,2048]{1,0:T(8,128)(2,1)} async-done(((bf16[1024,2048]{1,0:T(8,128)(2,1)}), bf16[128,2048]{1,0:T(8,128)(2,1)}) %reduce-scatter.5.cloned.1.call-update) | async-done | bytes 524304 | tf_op jit(solution)/shard_map/reduce_scatter | solution.py:214
  302.5 1.3 fusion.46
  303.8 1.4 multiply_reduce_fusion.1
  305.2 2.2 add_convert_fusion
  (75 shorter events, 3.2 us)
Async XLA Ops:
  7.4 106.8 %copy-start = (bf16[512,2048]{1,0:T(8,128)(2,1)S(1)}, bf16[512,2048]{1,0:T(8,128)(2,1)}, u32[]{:S(2)}) copy-start(bf16[512,2048]{1,0:T(8,128)(2,1)} %param.24) | copy-start | bytes 6291460
  7.4 47.7 %all-gather.13.cloned.1.call-start = ((), (), s32[]{:S(2)}) async-start(), calls=%async_computation.7 | async-start | bytes 1310720 | tf_op jit(solution)/shard_map/all_gather | solution.py:40
  10.4 5.3 %copy-start.4 = (bf16[1024,512]{1,0:T(8,128)(2,1)S(1)}, bf16[1024,512]{1,0:T(8,128)(2,1)}, u32[]{:S(2)}) copy-start(bf16[1024,512]{1,0:T(8,128)(2,1)} %param.20) | copy-start | bytes 3145732
  14.9 0.8 copy-start.3
  17.7 10.6 %copy-start.14 = (u32[128]{0:T(128)S(1)}, u32[128]{0:T(128)}, u32[]{:S(2)}) copy-start(u32[128]{0:T(128)} %constant.99) | copy-start | bytes 1540
  17.7 41.3 %copy-start.13 = (u32[128]{0:T(128)S(1)}, u32[128]{0:T(128)}, u32[]{:S(2)}) copy-start(u32[128]{0:T(128)} %constant.104) | copy-start | bytes 1540
  28.3 55.6 %all-gather.7.cloned.1.call-start = ((), (), s32[]{:S(2)}) async-start(), calls=%async_computation.2 | async-start | bytes 1310720 | tf_op jit(solution)/shard_map/all_gather | solution.py:40
  59.0 98.4 %reduce-scatter.3.cloned.1.call-start = ((), (), s32[]{:S(2)}) async-start(), calls=%async_computation.3 | async-start | bytes 4718592 | tf_op jit(solution)/shard_map/reduce_scatter | solution.py:193
  109.7 2.2 copy-start.1
  118.5 0.9 copy-start.5
  118.5 1.0 copy-start.6
  118.5 1.1 copy-start.7
  118.5 2.1 copy-start.9
  118.5 2.1 copy-start.10
  118.5 81.2 %all-gather.11.cloned.1.call-start = ((), (), s32[]{:S(2)}) async-start(), calls=%async_computation.5 | async-start | bytes 9191424 | tf_op jit(solution)/shard_map/all_gather | solution.py:20
  119.6 43.5 %copy-start.8 = (f32[2,3,704]{2,0,1:T(2,128)S(1)}, f32[2,3,704]{2,0,1:T(2,128)}, u32[]{:S(2)}) copy-start(f32[2,3,704]{2,0,1:T(2,128)} %param.29) | copy-start | bytes 50692
  120.5 111.9 %all-gather.9.cloned.1.call-start = ((), (), s32[]{:S(2)}) async-start(), calls=%async_computation.4 | async-start | bytes 4718592 | tf_op jit(solution)/shard_map/all_gather | solution.py:202
  162.8 139.7 %reduce-scatter.5.cloned.1.call-start = ((), (), s32[]{:S(2)}) async-start(), calls=%async_computation.6 | async-start | bytes 4718592 | tf_op jit(solution)/shard_map/reduce_scatter | solution.py:214
  232.4 6.5 %copy-start.12 = (bf16[1024,2048]{1,0:T(8,128)(2,1)S(1)}, bf16[1024,2048]{1,0:T(8,128)(2,1)}, u32[]{:S(2)}) copy-start(bf16[1024,2048]{1,0:T(8,128)(2,1)} %all-gather.9.cloned.1.call-done) | copy-start | bytes 12582916
  239.0 8.9 %copy-start.11 = (f32[2,704]{1,0:T(2,128)S(1)}, f32[2,704]{1,0:T(2,128)}, u32[]{:S(2)}) copy-start(f32[2,704]{1,0:T(2,128)} %param.30) | copy-start | bytes 16900
  244.3 7.6 %collective-permute-start = (bf16[4,704]{0,1:T(8,128)(2,1)S(1)}, bf16[4,704]{0,1:T(8,128)(2,1)S(1)}, u32[]{:S(2)}, u32[]{:S(2)}) collective-permute-start(bf16[4,704]{0,1:T(8,128)(2,1)S(1)} %pad_maximum_fusion.1), channel_id=1, source_target_pairs={{0,8},{8,16},{16,24},{24,32},{32,40},{40,48},{48,56},{56,64},{64,7... | collective-permute-start | bytes 16904 | tf_op jit(solution)/shard_map/ppermute | solution.py:58
  263.5 39.0 %copy-start.2 = (bf16[128,2048]{1,0:T(8,128)(2,1)S(1)}, bf16[128,2048]{1,0:T(8,128)(2,1)}, u32[]{:S(2)}) copy-start(bf16[128,2048]{1,0:T(8,128)(2,1)} %add_convert_fusion.1) | copy-start | bytes 1572868
Sparse Core Ops, SparseCore 0:
  28.4 26.5 all-gather.12
  59.1 24.6 all-gather.6
  118.7 38.6 reduce-scatter.2
  263.7 38.7 reduce-scatter.4
Sparse Core Ops, SparseCore 1:
  121.1 78.5 all-gather.10
  201.3 31.1 all-gather.8
